TPU v7x, 32 devices: a whole 2x2x4 slice. The times are simulated.
32 devices in a mesh: ep: 8 (over z, y), tp: 4 (over x, core).
Axes of the slice: x: 2, y: 2, z: 4, core: 2. Of those that a mesh axis runs over, the one named last changes fastest.
Arguments:
- tokens: bfloat16 [2048, 1024], P('ep'), may hold values from -6 to 6
- cotangent: bfloat16 [2048, 1024], P('ep'), may hold values from -1.5 to 1.5
- routing: int32 [2048, 2], P('ep'), may hold values from 0 to 15, all different within a row; in each aligned block of 256 rows (0 to 255, 256 to 511, ...) at most 96 rows name the same one
- gate_weights: float32 [2048, 2], P('ep'), may hold values from 0.1 to 0.9
- gate_proj: bfloat16 [16, 1024, 512], P('ep', None, 'tp'), may hold values from -0.1875 to 0.1875
- up_proj: bfloat16 [16, 1024, 512], P('ep', None, 'tp'), may hold values from -0.1875 to 0.1875
- down_proj: bfloat16 [16, 512, 1024], P('ep', 'tp'), may hold values from -0.25 to 0.25
Outputs:
- tokens_grad: bfloat16 [2048, 1024], P('ep')
- gates_grad: float32 [2048, 2], P('ep')
- gate_proj_grad: float32 [16, 1024, 512], P('ep', None, 'tp')
- up_proj_grad: float32 [16, 1024, 512], P('ep', None, 'tp')
- down_proj_grad: float32 [16, 512, 1024], P('ep', 'tp')
Inputs may be any that keep to these rules, and one draw needn't show every extreme that they name: `routing`: each row names 2 different experts; every expert is named by some row; within each aligned block of 256 rows (the tokens of one index of ep) no expert is named by more than 96 rows, a bound that some block reaches.
All inputs are finite; a program needn't handle non-finite values.
Results may differ from a plain program's by a relative error of at most 0.0015.
Values may be sent and summed in bfloat16 or wider, within the bound.
A program may use at most 128 MiB of HBM per device.

v0:
```python
import jax
import jax.numpy as jnp
from jax import lax
from jax.sharding import PartitionSpec as P


def expert_terms(expert_rows, expert_scaled, gate_proj, up_proj, down_proj):
    gate_pre = jnp.einsum(
        "erd,edf->erf", expert_rows, gate_proj, preferred_element_type=jnp.float32
    ).astype(jnp.bfloat16)
    up_pre = jnp.einsum(
        "erd,edf->erf", expert_rows, up_proj, preferred_element_type=jnp.float32
    ).astype(jnp.bfloat16)
    gate_pre, up_pre = lax.optimization_barrier((gate_pre, up_pre))
    hidden_grad = jnp.einsum(
        "erd,efd->erf", expert_scaled, down_proj, preferred_element_type=jnp.float32
    )
    gate_wide = gate_pre.astype(jnp.float32)
    up_wide = up_pre.astype(jnp.float32)
    sigmoid_gate = jax.nn.sigmoid(gate_wide)
    activated = gate_wide * sigmoid_gate
    hidden = activated * up_wide
    product = jnp.sum(hidden_grad * hidden, axis=-1)
    gate_pre_grad = (
        hidden_grad * up_wide * sigmoid_gate * (1.0 + gate_wide * (1.0 - sigmoid_gate))
    ).astype(jnp.bfloat16)
    up_pre_grad = (hidden_grad * activated).astype(jnp.bfloat16)
    input_grad = jnp.einsum(
        "erf,edf->erd", gate_pre_grad, gate_proj, preferred_element_type=jnp.float32
    )
    input_grad = input_grad + jnp.einsum(
        "erf,edf->erd", up_pre_grad, up_proj, preferred_element_type=jnp.float32
    )
    down_grad = jnp.einsum(
        "erf,erd->efd",
        hidden.astype(jnp.bfloat16),
        expert_scaled,
        preferred_element_type=jnp.float32,
    )
    gate_grad = jnp.einsum(
        "erd,erf->edf", expert_rows, gate_pre_grad, preferred_element_type=jnp.float32
    )
    up_grad = jnp.einsum(
        "erd,erf->edf", expert_rows, up_pre_grad, preferred_element_type=jnp.float32
    )
    return (input_grad, product, gate_grad, up_grad, down_grad)


def shards(tokens, cotangent, routing, gate_weights, gate_proj, up_proj, down_proj):
    token_count, model_width = tokens.shape
    top_count = routing.shape[1]
    local_experts = gate_proj.shape[0]
    groups = lax.axis_size("ep")
    members = lax.axis_size("tp")
    experts = local_experts * groups
    capacity = members * (
        (3 * token_count * top_count + experts * members - 1) // (experts * members)
    )
    slot_count = experts * capacity
    pair_count = token_count * top_count
    pair_expert = routing.reshape(pair_count)
    onehot = (pair_expert[:, None] == jnp.arange(experts, dtype=jnp.int32)[None, :]).astype(
        jnp.int32
    )
    position = jnp.sum(jnp.cumsum(onehot, axis=0) * onehot, axis=1) - 1
    pair_slot = pair_expert * capacity + position
    pair_number = jnp.arange(pair_count, dtype=jnp.int32)
    owner_pair = jnp.zeros((slot_count,), jnp.int32).at[pair_slot].set(pair_number)
    filled = jnp.zeros((slot_count,), jnp.int32).at[pair_slot].set(1) > 0
    owner_token = owner_pair // top_count
    slot_weight = jnp.where(filled, gate_weights.reshape(pair_count)[owner_pair], 0.0)
    send_rows = jnp.where(filled[:, None], tokens[owner_token], jnp.zeros((), jnp.bfloat16))
    send_scaled = (slot_weight[:, None] * cotangent[owner_token].astype(jnp.float32)).astype(
        jnp.bfloat16
    )
    layout = (groups, local_experts, capacity, model_width)
    send_rows = send_rows.reshape(layout)
    send_scaled = send_scaled.reshape(layout)
    quarter = capacity // members
    quarter_start = lax.axis_index("tp") * quarter
    part_rows = lax.dynamic_slice_in_dim(send_rows, quarter_start, quarter, 2)
    part_scaled = lax.dynamic_slice_in_dim(send_scaled, quarter_start, quarter, 2)
    landed = (
        lax.all_to_all(part_rows, "ep", split_axis=0, concat_axis=0, tiled=True),
        lax.all_to_all(part_scaled, "ep", split_axis=0, concat_axis=0, tiled=True),
    )
    recv_rows, recv_scaled = (
        lax.all_gather(landed[0], "tp", axis=2, tiled=True),
        lax.all_gather(landed[1], "tp", axis=2, tiled=True),
    )
    expert_rows = recv_rows.transpose(1, 0, 2, 3).reshape(
        local_experts, groups * capacity, model_width
    )
    expert_scaled = recv_scaled.transpose(1, 0, 2, 3).reshape(
        local_experts, groups * capacity, model_width
    )
    input_grad, product, gate_grad, up_grad, down_grad = expert_terms(
        expert_rows, expert_scaled, gate_proj, up_proj, down_proj
    )
    input_grad = input_grad.reshape(local_experts, groups, capacity, model_width).transpose(
        1, 0, 2, 3
    )
    product = product.reshape(local_experts, groups, capacity).transpose(1, 0, 2)
    back_grad, back_product = (
        lax.all_to_all(input_grad, "ep", split_axis=0, concat_axis=0, tiled=True),
        lax.all_to_all(product, "ep", split_axis=0, concat_axis=0, tiled=True),
    )
    local_slot = position
    present = (local_slot >= 0) & (local_slot < capacity)
    back_index = pair_expert * capacity + jnp.clip(local_slot, 0, capacity - 1)
    pair_grad = jnp.where(
        present[:, None], back_grad.reshape(experts * capacity, model_width)[back_index], 0.0
    )
    pair_product = jnp.where(present, back_product.reshape(experts * capacity)[back_index], 0.0)
    token_grad = jnp.sum(pair_grad.reshape(token_count, top_count, model_width), axis=1)
    total_grad, total_product = lax.psum((token_grad, pair_product), "tp")
    tokens_grad = total_grad.astype(jnp.bfloat16)
    gates_grad = (total_product / gate_weights.reshape(pair_count)).reshape(token_count, top_count)
    return (tokens_grad, gates_grad, gate_grad, up_grad, down_grad)


def solution(mesh):
    in_specs = (
        P("ep", None),
        P("ep", None),
        P("ep", None),
        P("ep", None),
        P("ep", None, "tp"),
        P("ep", None, "tp"),
        P("ep", "tp", None),
    )
    out_specs = (
        P("ep", None),
        P("ep", None),
        P("ep", None, "tp"),
        P("ep", None, "tp"),
        P("ep", "tp", None),
    )
    return jax.shard_map(shards, mesh=mesh, in_specs=in_specs, out_specs=out_specs, check_vma=False)
```

profile of v0, /device:TPU:0, one launch (start us, length us, event | category | flops | bytes accessed | tf_op | source)
XLA Modules:
  0.0 324.4 jit_solution(3575784898565409781)
XLA Ops:
  9.4 1.2 reduce-window.6
  10.9 2.5 scatter_custom_fusion.1
  13.4 2.5 scatter_custom_fusion
  15.9 0.8 copy.66
  16.9 9.5 %gather_fusion = f32[1536]{0:T(1024)S(1)} fusion(f32[512]{0:T(512)S(1)} %reshape.148, s32[2048]{0:T(1024)S(1)} %get-tuple-element.38), kind=kCustom, calls=%fused_computation | custom fusion | bytes 18432 | tf_op jit(solution)/shard_map/gather | solution.py:71
  26.5 5.8 %gather_fusion.2 = bf16[1536,1024]{1,0:T(8,128)(2,1)} fusion(bf16[256,1024]{1,0:T(8,128)(2,1)S(1)} %copy-done.1, s32[2048]{0:T(1024)S(1)} %get-tuple-element.37), kind=kCustom, calls=%fused_computation.2 | custom fusion | bytes 6297600 | tf_op jit(solution)/shard_map/gather | solution.py:72
  32.3 1.4 dynamic-slice_select_fusion
  33.7 27.4 %all_to_all.20 = bf16[8,2,24,1024]{3,2,1,0:T(8,128)(2,1)} all-to-all(bf16[8,2,24,1024]{3,2,1,0:T(8,128)(2,1)S(1)} %dynamic-slice_select_fusion), channel_id=1, replica_groups=mesh['ep'=8,'tp'=4] {'ep'}, dimensions={0} | all-to-all | bytes 1572864 | tf_op jit(solution)/shard_map/all_to_all | solution.py:84
  61.3 5.8 %gather_fusion.1 = bf16[1536,1024]{1,0:T(8,128)(2,1)} fusion(bf16[256,1024]{1,0:T(8,128)(2,1)S(1)} %copy-done.2, s32[2048]{0:T(1024)S(1)} %get-tuple-element.37), kind=kCustom, calls=%fused_computation.1 | custom fusion | bytes 6297600 | tf_op jit(solution)/shard_map/gather | solution.py:73
  67.1 1.4 fusion
  68.5 23.2 %all_to_all.21 = bf16[8,2,24,1024]{3,2,1,0:T(8,128)(2,1)} all-to-all(bf16[8,2,24,1024]{3,2,1,0:T(8,128)(2,1)S(1)} %fusion), channel_id=1, replica_groups=mesh['ep'=8,'tp'=4] {'ep'}, dimensions={0} | all-to-all | bytes 1572864 | tf_op jit(solution)/shard_map/all_to_all | solution.py:85
  91.8 2.4 copy.68
  94.2 1.2 convolution_convert_fusion
  95.9 1.2 convolution_convert_fusion.1
  97.1 22.4 %all-gather.3.cloned.1.call-done = bf16[8,2,96,1024]{3,2,1,0:T(8,128)(2,1)} async-done(((bf16[8,2,24,1024]{3,2,1,0:T(8,128)(2,1)}), bf16[8,2,96,1024]{3,2,1,0:T(8,128)(2,1)}) %all-gather.3.cloned.1.call-update) | async-done | bytes 3145744 | tf_op jit(solution)/shard_map/all_gather | solution.py:89
  119.5 2.4 copy.67
  121.9 1.4 multiply_reduce_fusion
  124.2 5.5 %all-to-all-start.3 = ((f32[8,2,96]{2,1,0:T(2,128)}), f32[8,2,96]{2,1,0:T(2,128)S(1)}, u32[]{:S(2)}, u32[]{:S(2)}) async-start(f32[8,2,96]{2,1,0:T(2,128)} %copy.74), calls=%async_computation.3 | async-start | bytes 16384 | tf_op jit(solution)/shard_map/all_to_all | solution.py:106
  129.7 1.0 fusion.21
  130.7 1.1 convolution_add_fusion
  131.8 3.2 copy.91
  135.1 1.2 all-to-all-done.3
  136.2 4.8 %all-to-all-start.2 = ((f32[8,2,96,1024]{3,2,1,0:T(8,128)}), f32[8,2,96,1024]{3,2,1,0:T(8,128)}, u32[]{:S(2)}, u32[]{:S(2)}) async-start(f32[8,2,96,1024]{3,2,1,0:T(8,128)} %bitcast.50), calls=%async_computation.2 | async-start | bytes 12582912 | tf_op jit(solution)/shard_map/all_to_all | solution.py:105
  141.1 4.4 %fusion.22 = f32[2,1024,128]{2,1,0:T(8,128)} fusion(bf16[2,768,1024]{2,1,0:T(8,128)(2,1)} %bitcast.48, bf16[2,768,128]{1,2,0:T(8,128)(2,1)S(1)} %get-tuple-element.31), kind=kOutput, calls=%fused_computation.67 | convolution fusion | flops 402653184 | bytes 4587520 | tf_op jit(solution)/shard_map/erd,erf->edf/dot_general | solution.py:40
  145.4 1.8 fusion.9
  147.7 2.4 fusion.20
  150.1 3.1 gather_fusion.4
  153.4 125.7 %all-to-all-done.2 = f32[8,2,96,1024]{3,2,1,0:T(8,128)} async-done(((f32[8,2,96,1024]{3,2,1,0:T(8,128)}), f32[8,2,96,1024]{3,2,1,0:T(8,128)}, u32[]{:S(2)}, u32[]{:S(2)}) %all-to-all-start.2) | async-done | bytes 6291488 | tf_op jit(solution)/shard_map/all_to_all | solution.py:105
  279.1 5.6 %gather_fusion.3 = f32[512,1024]{1,0:T(8,128)S(1)} fusion(f32[1536,1024]{1,0:T(8,128)} %bitcast.11, s32[1024]{0:T(1024)S(1)} %pad_clamp_fusion.2), kind=kCustom, calls=%fused_computation.3 | custom fusion | bytes 4196352 | tf_op jit(solution)/shard_map/gather | solution.py:112
  284.7 2.3 gather.24
  287.0 4.1 %select_reduce_fusion = f32[256,1024]{1,0:T(8,128)S(1)} fusion(f32[256,2,1024]{2,1,0:T(2,128)} %gather.24, pred[256,2]{1,0:T(8,128)(4,1)S(1)} %and.17), kind=kLoop, calls=%fused_computation.9 | loop fusion | flops 786432 | bytes 3146240 | tf_op jit(solution)/shard_map/reduce_sum | solution.py:115
  291.2 25.5 %all-reduce.2 = (bf16[256,1024]{1,0:T(8,128)(2,1)}, f32[512]{0:T(512)S(1)}) all-reduce(f32[256,1024]{1,0:T(8,128)S(1)} %select_reduce_fusion, f32[512]{0:T(512)S(1)} %get-tuple-element.26), channel_id=1, replica_groups=mesh['ep'=8,'tp'=4] {'tp'}, use_global_device_ids=true, to_apply=%region_6.7 | all-reduce | flops 262656 | bytes 1576960 | tf_op jit(solution)/shard_map/psum | solution.py:116
  (55 shorter events, 6.1 us)
Async XLA Ops:
  7.2 88.7 %copy-start = (bf16[2,1024,128]{2,1,0:T(8,128)(2,1)S(1)}, bf16[2,1024,128]{2,1,0:T(8,128)(2,1)}, u32[]{:S(2)}) copy-start(bf16[2,1024,128]{2,1,0:T(8,128)(2,1)} %param.11) | copy-start | bytes 1572868
  7.2 84.6 %all-gather.5.cloned.1.call-start = ((), (), s32[]{:S(2)}) async-start(), calls=%async_computation.5 | async-start | bytes 3932160 | tf_op jit(solution)/shard_map/all_gather | solution.py:88
  16.9 9.7 %copy-start.1 = (bf16[256,1024]{1,0:T(8,128)(2,1)S(1)}, bf16[256,1024]{1,0:T(8,128)(2,1)}, u32[]{:S(2)}) copy-start(bf16[256,1024]{1,0:T(8,128)(2,1)} %param.7) | copy-start | bytes 1572868
  32.3 28.9 %copy-start.2 = (bf16[256,1024]{1,0:T(8,128)(2,1)S(1)}, bf16[256,1024]{1,0:T(8,128)(2,1)}, u32[]{:S(2)}) copy-start(bf16[256,1024]{1,0:T(8,128)(2,1)} %param.8) | copy-start | bytes 1572868
  61.1 58.3 %all-gather.3.cloned.1.call-start = ((), (), s32[]{:S(2)}) async-start(), calls=%async_computation.4 | async-start | bytes 3932160 | tf_op jit(solution)/shard_map/all_gather | solution.py:89
  91.8 2.4 copy-start.7
  94.2 1.7 copy-start.3
  119.5 2.4 copy-start.8
  121.8 1.7 copy-start.5
  124.2 12.0 %all-to-all-start.3 = ((f32[8,2,96]{2,1,0:T(2,128)}), f32[8,2,96]{2,1,0:T(2,128)S(1)}, u32[]{:S(2)}, u32[]{:S(2)}) async-start(f32[8,2,96]{2,1,0:T(2,128)} %copy.74), calls=%async_computation.3 | async-start | bytes 16384 | tf_op jit(solution)/shard_map/all_to_all | solution.py:106
  136.2 142.9 %all-to-all-start.2 = ((f32[8,2,96,1024]{3,2,1,0:T(8,128)}), f32[8,2,96,1024]{3,2,1,0:T(8,128)}, u32[]{:S(2)}, u32[]{:S(2)}) async-start(f32[8,2,96,1024]{3,2,1,0:T(8,128)} %bitcast.50), calls=%async_computation.2 | async-start | bytes 12582912 | tf_op jit(solution)/shard_map/all_to_all | solution.py:105
  141.1 4.4 %copy-start.6 = (bf16[2,8,96,1024]{3,2,1,0:T(8,128)(2,1)S(1)}, bf16[2,8,96,1024]{3,2,1,0:T(8,128)(2,1)}, u32[]{:S(2)}) copy-start(bf16[2,8,96,1024]{3,2,1,0:T(8,128)(2,1)} %copy-done.5) | copy-start | bytes 9437188
  145.4 2.2 copy-start.4
Sparse Core Ops, SparseCore 0:
  61.2 27.5 all-gather.4
  91.9 27.4 all-gather.2
where the time goes:
time: 325 us; the launch traced here: 324 us
  waiting for transfers between devices  149 us (46%)
  blocking collectives  76.2 us (23%)
  local copies, waits for them, and re-layouts  50.8 us (16%)
  between operations  14.4 us (4%)
  matrix products  14.3 us (4%)
  starting transfers between devices  10.4 us (3%)
  other arithmetic  8.97 us (3%)
    all_to_all x1, waiting for transfers between devices, shards(): lax.all_to_all(input_grad, 'ep', split_axis=0, concat_axis=0, tiled=True)  126 us
    all_to_all x1, blocking collectives, shards(): lax.all_to_all(part_rows, 'ep', split_axis=0, concat_axis=0, tiled=True)  27.4 us
    psum x1, blocking collectives, shards(): total_grad, total_product = lax.psum((token_grad, pair_product), 'tp')  25.5 us
    all_to_all x1, blocking collectives, shards(): lax.all_to_all(part_scaled, 'ep', split_axis=0, concat_axis=0, tiled=True)  23.2 us
    all_gather x1, waiting for transfers between devices, shards(): lax.all_gather(landed[1], 'tp', axis=2, tiled=True)  22.4 us
    gather x1, local copies, waits for them, and re-layouts, shards(): gate_weights.reshape(pair_count)[owner_pair]  9.48 us
    gather x2, local copies, waits for them, and re-layouts, shards(): back_grad.reshape(experts * capacity, model_width)[back_index]  7.9 us
  transfers between devices with their start and end apart: 4, of which 3 were waited for; matrix products, arithmetic and copies ran while one was open for 9% of the time, Pallas kernels for 0%

commit v1 on v0

--- a/solution.py
+++ b/solution.py
@@ -86,7 +86,7 @@
     )
     recv_rows, recv_scaled = (
         lax.all_gather(landed[0], "tp", axis=2, tiled=True),
-        lax.all_gather(landed[1], "tp", axis=2, tiled=True),
+        jnp.concatenate(lax.all_gather(landed[1], "tp"), axis=2),
     )
     expert_rows = recv_rows.transpose(1, 0, 2, 3).reshape(
         local_experts, groups * capacity, model_width

time: 325 us -> 325 us (level)
  no operation moved by 1% of the time
where the time goes in v1:
time: 325 us; the launch traced here: 324 us
  waiting for transfers between devices  149 us (46%)
  blocking collectives  76.1 us (23%)
  local copies, waits for them, and re-layouts  50.8 us (16%)
  between operations  14.4 us (4%)
  matrix products  14.3 us (4%)
  starting transfers between devices  10.4 us (3%)
  other arithmetic  8.97 us (3%)
    all_to_all x1, waiting for transfers between devices, shards(): lax.all_to_all(input_grad, 'ep', split_axis=0, concat_axis=0, tiled=True)  126 us
    all_to_all x1, blocking collectives, shards(): lax.all_to_all(part_rows, 'ep', split_axis=0, concat_axis=0, tiled=True)  27.4 us
    psum x1, blocking collectives, shards(): total_grad, total_product = lax.psum((token_grad, pair_product), 'tp')  25.5 us
    all_to_all x1, blocking collectives, shards(): lax.all_to_all(part_scaled, 'ep', split_axis=0, concat_axis=0, tiled=True)  23.2 us
    all_gather x1, waiting for transfers between devices, shards(): lax.all_gather(landed[1], 'tp')  22.4 us
    gather x1, local copies, waits for them, and re-layouts, shards(): gate_weights.reshape(pair_count)[owner_pair]  9.48 us
    gather x2, local copies, waits for them, and re-layouts, shards(): back_grad.reshape(experts * capacity, model_width)[back_index]  7.9 us
  transfers between devices with their start and end apart: 4, of which 3 were waited for; matrix products, arithmetic and copies ran while one was open for 9% of the time, Pallas kernels for 0%

profile of v1, /device:TPU:0, one launch (start us, length us, event | category | flops | bytes accessed | tf_op | source)
XLA Modules:
  0.0 324.4 jit_solution(9123249410228681387)
XLA Ops:
  9.4 1.2 reduce-window.6
  10.9 2.5 scatter_custom_fusion.1
  13.4 2.5 scatter_custom_fusion
  15.9 0.8 copy.64
  16.9 9.5 %gather_fusion = f32[1536]{0:T(1024)S(1)} fusion(f32[512]{0:T(512)S(1)} %reshape.154, s32[2048]{0:T(1024)S(1)} %get-tuple-element.38), kind=kCustom, calls=%fused_computation | custom fusion | bytes 18432 | tf_op jit(solution)/shard_map/gather | solution.py:71
  26.5 5.8 %gather_fusion.2 = bf16[1536,1024]{1,0:T(8,128)(2,1)} fusion(bf16[256,1024]{1,0:T(8,128)(2,1)S(1)} %copy-done.1, s32[2048]{0:T(1024)S(1)} %get-tuple-element.37), kind=kCustom, calls=%fused_computation.2 | custom fusion | bytes 6297600 | tf_op jit(solution)/shard_map/gather | solution.py:72
  32.3 1.4 dynamic-slice_select_fusion
  33.7 27.4 %all_to_all.20 = bf16[8,2,24,1024]{3,2,1,0:T(8,128)(2,1)} all-to-all(bf16[8,2,24,1024]{3,2,1,0:T(8,128)(2,1)S(1)} %dynamic-slice_select_fusion), channel_id=1, replica_groups=mesh['ep'=8,'tp'=4] {'ep'}, dimensions={0} | all-to-all | bytes 1572864 | tf_op jit(solution)/shard_map/all_to_all | solution.py:84
  61.3 5.8 %gather_fusion.1 = bf16[1536,1024]{1,0:T(8,128)(2,1)} fusion(bf16[256,1024]{1,0:T(8,128)(2,1)S(1)} %copy-done.2, s32[2048]{0:T(1024)S(1)} %get-tuple-element.37), kind=kCustom, calls=%fused_computation.1 | custom fusion | bytes 6297600 | tf_op jit(solution)/shard_map/gather | solution.py:73
  67.1 1.4 fusion
  68.5 23.2 %all_to_all.21 = bf16[8,2,24,1024]{3,2,1,0:T(8,128)(2,1)} all-to-all(bf16[8,2,24,1024]{3,2,1,0:T(8,128)(2,1)S(1)} %fusion), channel_id=1, replica_groups=mesh['ep'=8,'tp'=4] {'ep'}, dimensions={0} | all-to-all | bytes 1572864 | tf_op jit(solution)/shard_map/all_to_all | solution.py:85
  91.8 2.4 copy.66
  94.2 1.2 convolution_convert_fusion
  95.9 1.2 convolution_convert_fusion.1
  97.1 22.4 %all-gather.6.cloned.1.call-done = bf16[32,2,24,1024]{3,2,1,0:T(8,128)(2,1)} async-done(((bf16[8,2,24,1024]{3,2,1,0:T(8,128)(2,1)}), bf16[32,2,24,1024]{3,2,1,0:T(8,128)(2,1)}) %all-gather.6.cloned.1.call-update) | async-done | bytes 3145744 | tf_op jit(solution)/shard_map/all_gather | solution.py:89
  119.5 2.4 copy.65
  121.9 1.4 multiply_reduce_fusion
  124.2 5.5 %all-to-all-start.3 = ((f32[8,2,96]{2,1,0:T(2,128)}), f32[8,2,96]{2,1,0:T(2,128)S(1)}, u32[]{:S(2)}, u32[]{:S(2)}) async-start(f32[8,2,96]{2,1,0:T(2,128)} %copy.72), calls=%async_computation.3 | async-start | bytes 16384 | tf_op jit(solution)/shard_map/all_to_all | solution.py:106
  129.7 1.0 fusion.21
  130.8 1.1 convolution_add_fusion
  131.8 3.2 copy.89
  135.1 1.2 all-to-all-done.3
  136.2 4.8 %all-to-all-start.2 = ((f32[8,2,96,1024]{3,2,1,0:T(8,128)}), f32[8,2,96,1024]{3,2,1,0:T(8,128)}, u32[]{:S(2)}, u32[]{:S(2)}) async-start(f32[8,2,96,1024]{3,2,1,0:T(8,128)} %bitcast.56), calls=%async_computation.2 | async-start | bytes 12582912 | tf_op jit(solution)/shard_map/all_to_all | solution.py:105
  141.1 4.4 %fusion.22 = f32[2,1024,128]{2,1,0:T(8,128)} fusion(bf16[2,768,1024]{2,1,0:T(8,128)(2,1)} %bitcast.54, bf16[2,768,128]{1,2,0:T(8,128)(2,1)S(1)} %get-tuple-element.31), kind=kOutput, calls=%fused_computation.67 | convolution fusion | flops 402653184 | bytes 4587520 | tf_op jit(solution)/shard_map/erd,erf->edf/dot_general | solution.py:40
  145.5 1.8 fusion.9
  147.7 2.4 fusion.20
  150.1 3.1 gather_fusion.4
  153.5 125.7 %all-to-all-done.2 = f32[8,2,96,1024]{3,2,1,0:T(8,128)} async-done(((f32[8,2,96,1024]{3,2,1,0:T(8,128)}), f32[8,2,96,1024]{3,2,1,0:T(8,128)}, u32[]{:S(2)}, u32[]{:S(2)}) %all-to-all-start.2) | async-done | bytes 6291488 | tf_op jit(solution)/shard_map/all_to_all | solution.py:105
  279.1 5.6 %gather_fusion.3 = f32[512,1024]{1,0:T(8,128)S(1)} fusion(f32[1536,1024]{1,0:T(8,128)} %bitcast.14, s32[1024]{0:T(1024)S(1)} %pad_clamp_fusion.2), kind=kCustom, calls=%fused_computation.3 | custom fusion | bytes 4196352 | tf_op jit(solution)/shard_map/gather | solution.py:112
  284.8 2.3 gather.24
  287.0 4.1 %select_reduce_fusion = f32[256,1024]{1,0:T(8,128)S(1)} fusion(f32[256,2,1024]{2,1,0:T(2,128)} %gather.24, pred[256,2]{1,0:T(8,128)(4,1)S(1)} %and.17), kind=kLoop, calls=%fused_computation.9 | loop fusion | flops 786432 | bytes 3146240 | tf_op jit(solution)/shard_map/reduce_sum | solution.py:115
  291.2 25.5 %all-reduce.2 = (bf16[256,1024]{1,0:T(8,128)(2,1)}, f32[512]{0:T(512)S(1)}) all-reduce(f32[256,1024]{1,0:T(8,128)S(1)} %select_reduce_fusion, f32[512]{0:T(512)S(1)} %get-tuple-element.26), channel_id=1, replica_groups=mesh['ep'=8,'tp'=4] {'tp'}, use_global_device_ids=true, to_apply=%region_6.7 | all-reduce | flops 262656 | bytes 1576960 | tf_op jit(solution)/shard_map/psum | solution.py:116
  (55 shorter events, 6.1 us)
Async XLA Ops:
  7.2 88.7 %copy-start = (bf16[2,1024,128]{2,1,0:T(8,128)(2,1)S(1)}, bf16[2,1024,128]{2,1,0:T(8,128)(2,1)}, u32[]{:S(2)}) copy-start(bf16[2,1024,128]{2,1,0:T(8,128)(2,1)} %param.11) | copy-start | bytes 1572868
  7.2 84.6 %all-gather.4.cloned.1.call-start = ((), (), s32[]{:S(2)}) async-start(), calls=%async_computation.4 | async-start | bytes 3932160 | tf_op jit(solution)/shard_map/all_gather | solution.py:88
  16.9 9.7 %copy-start.1 = (bf16[256,1024]{1,0:T(8,128)(2,1)S(1)}, bf16[256,1024]{1,0:T(8,128)(2,1)}, u32[]{:S(2)}) copy-start(bf16[256,1024]{1,0:T(8,128)(2,1)} %param.7) | copy-start | bytes 1572868
  32.3 28.9 %copy-start.2 = (bf16[256,1024]{1,0:T(8,128)(2,1)S(1)}, bf16[256,1024]{1,0:T(8,128)(2,1)}, u32[]{:S(2)}) copy-start(bf16[256,1024]{1,0:T(8,128)(2,1)} %param.8) | copy-start | bytes 1572868
  61.1 58.3 %all-gather.6.cloned.1.call-start = ((), (), s32[]{:S(2)}) async-start(), calls=%async_computation.5 | async-start | bytes 3932160 | tf_op jit(solution)/shard_map/all_gather | solution.py:89
  91.8 2.4 copy-start.7
  94.2 1.7 copy-start.3
  119.5 2.4 copy-start.8
  121.9 1.7 copy-start.5
  124.2 12.0 %all-to-all-start.3 = ((f32[8,2,96]{2,1,0:T(2,128)}), f32[8,2,96]{2,1,0:T(2,128)S(1)}, u32[]{:S(2)}, u32[]{:S(2)}) async-start(f32[8,2,96]{2,1,0:T(2,128)} %copy.72), calls=%async_computation.3 | async-start | bytes 16384 | tf_op jit(solution)/shard_map/all_to_all | solution.py:106
  136.2 142.9 %all-to-all-start.2 = ((f32[8,2,96,1024]{3,2,1,0:T(8,128)}), f32[8,2,96,1024]{3,2,1,0:T(8,128)}, u32[]{:S(2)}, u32[]{:S(2)}) async-start(f32[8,2,96,1024]{3,2,1,0:T(8,128)} %bitcast.56), calls=%async_computation.2 | async-start | bytes 12582912 | tf_op jit(solution)/shard_map/all_to_all | solution.py:105
  141.1 4.4 %copy-start.6 = (bf16[8,2,4,24,1024]{4,3,2,0,1:T(8,128)(2,1)S(1)}, bf16[8,2,4,24,1024]{4,3,2,0,1:T(8,128)(2,1)}, u32[]{:S(2)}) copy-start(bf16[8,2,4,24,1024]{4,3,2,0,1:T(8,128)(2,1)} %copy-done.5) | copy-start | bytes 9437188
  145.5 2.2 copy-start.4
Sparse Core Ops, SparseCore 0:
  61.2 27.5 all-gather.3
  91.9 27.4 all-gather.5
